TPU v7x, 32 devices: a whole 2x2x4 slice. The times are simulated.
32 devices in a mesh: tp: 8 (over z, y), dp: 4 (over x, core).
Axes of the slice: x: 2, y: 2, z: 4, core: 2. Of those that a mesh axis runs over, the one named last changes fastest.
Arguments:
- tokens: bfloat16 [32, 4096], P('dp', 'tp'), may hold values from -6 to 6
- norm_gain: float32 [2, 4096], replicated, may hold values from 0.1 to 1.9
- w_query: bfloat16 [2, 4096, 2048], P(None, 'dp', 'tp'), may hold values from -0.09375 to 0.09375
- w_key: bfloat16 [2, 4096, 2048], P(None, 'dp', 'tp'), may hold values from -0.09375 to 0.09375
- w_value: bfloat16 [2, 4096, 4096], P(None, 'dp', 'tp'), may hold values from -0.09375 to 0.09375
- w_outgate: bfloat16 [2, 4096, 4096], P(None, 'dp', 'tp'), may hold values from -0.09375 to 0.09375
- w_ingate: bfloat16 [2, 4096, 16], P(None, 'dp'), may hold values from -0.09375 to 0.09375
- w_forget: bfloat16 [2, 4096, 16], P(None, 'dp'), may hold values from -0.09375 to 0.09375
- forget_bias: float32 [2, 16], replicated, may hold values from -2 to 5
- w_output: bfloat16 [2, 4096, 4096], P(None, 'dp', 'tp'), may hold values from -0.09375 to 0.09375
- mem_state: float32 [2, 32, 4096, 128], P(None, 'dp', 'tp'), may hold values from -0.8 to 0.8
- norm_state: float32 [2, 32, 16, 128], P(None, 'dp'), may hold values from -0.8 to 0.8
- max_state: float32 [2, 32, 16], P(None, 'dp'), may hold values from -4 to 4
Outputs:
- mixed: bfloat16 [32, 4096], P('dp', 'tp')
- new_memory: float32 [2, 32, 4096, 128], P(None, 'dp', 'tp')
- new_normaliser: float32 [2, 32, 16, 128], P(None, 'dp')
- new_stabiliser: float32 [2, 32, 16], P(None, 'dp')
All inputs are finite; a program needn't handle non-finite values.
Results may differ from a plain program's by a relative error of at most 0.013.
Values may be sent and summed in bfloat16 or wider, within the bound.
A program may use at most 128 MiB of HBM per device.

v0:
```python
import jax
import jax.numpy as jnp
from jax import lax
from jax.sharding import PartitionSpec as P

H = 16
DK = 128
DV = 256
BLOCKS = 2


EPSILON = 1e-06


def full_rows(shard):
    return lax.all_gather(shard, "tp", axis=1, tiled=True)


def fold_with(activations, pieces):
    return tuple(
        (jnp.dot(activations, piece, preferred_element_type=jnp.float32) for piece in pieces)
    )


def shards(
    tokens,
    norm_gain,
    w_query,
    w_key,
    w_value,
    w_outgate,
    w_ingate,
    w_forget,
    forget_bias,
    w_output,
    mem_state,
    norm_state,
    max_state,
):
    seq_count = tokens.shape[0]
    value_cols = w_value.shape[2]
    column_head = (
        lax.axis_index("tp") * value_cols + jnp.arange(value_cols, dtype=jnp.int32)
    ) // DV
    current = tokens
    memories, normalisers, maxima = ([], [], [])
    for layer in range(BLOCKS):
        whole = full_rows(current)
        wide = whole.astype(jnp.float32)
        scale = lax.rsqrt(jnp.mean(wide * wide, axis=-1, keepdims=True) + EPSILON)
        normed = (wide * scale * norm_gain[layer]).astype(jnp.bfloat16)
        parts = fold_with(
            normed,
            (
                lax.all_gather(w_query[layer], "dp", axis=0, tiled=True),
                lax.all_gather(w_key[layer], "dp", axis=0, tiled=True),
                lax.all_gather(w_value[layer], "dp", axis=0, tiled=True),
                lax.all_gather(w_outgate[layer], "dp", axis=0, tiled=True),
                lax.all_gather(w_ingate[layer], "dp", axis=0, tiled=True),
                lax.all_gather(w_forget[layer], "dp", axis=0, tiled=True),
            ),
        )
        query = parts[0].astype(jnp.bfloat16)
        keys = parts[1].astype(jnp.bfloat16)
        values = parts[2].astype(jnp.bfloat16)
        outgate = parts[3].astype(jnp.bfloat16)
        in_pre = parts[4]
        forget_pre = parts[5]
        query_all, keys_all = (
            lax.all_gather(query, "tp", axis=1, tiled=True),
            lax.all_gather(keys, "tp", axis=1, tiled=True),
        )
        log_forget = jax.nn.log_sigmoid(forget_pre + forget_bias[layer])
        new_max = jnp.maximum(log_forget + max_state[layer], in_pre)
        carried = jnp.exp(log_forget + max_state[layer] - new_max)
        fresh = jnp.exp(in_pre - new_max)
        query_heads = query_all.astype(jnp.float32).reshape(seq_count, H, DK)
        key_heads = keys_all.astype(jnp.float32).reshape(seq_count, H, DK) * DK ** (-0.5)
        new_norm = carried[:, :, None] * norm_state[layer] + fresh[:, :, None] * key_heads
        divisor = jnp.maximum(jnp.abs(jnp.sum(new_norm * query_heads, axis=-1)), 1.0)
        query_cols = jnp.take(query_heads, column_head, axis=1)
        key_cols = jnp.take(key_heads, column_head, axis=1)
        carried_cols = jnp.take(carried, column_head, axis=1)
        fresh_cols = jnp.take(fresh, column_head, axis=1)
        divisor_cols = jnp.take(divisor, column_head, axis=1)
        value_wide = values.astype(jnp.float32)
        new_state = (
            carried_cols[:, :, None] * mem_state[layer]
            + fresh_cols[:, :, None] * value_wide[:, :, None] * key_cols
        )
        readout = jnp.sum(new_state * query_cols, axis=-1) / divisor_cols
        gated = (jax.nn.sigmoid(outgate.astype(jnp.float32)) * readout).astype(jnp.bfloat16)
        gated_rows = full_rows(gated)
        update = jnp.dot(
            gated_rows,
            lax.all_gather(w_output[layer], "dp", axis=0, tiled=True),
            preferred_element_type=jnp.float32,
        )
        current = (current.astype(jnp.float32) + update).astype(jnp.bfloat16)
        memories.append(new_state)
        normalisers.append(new_norm)
        maxima.append(new_max)
    return (current, jnp.stack(memories), jnp.stack(normalisers), jnp.stack(maxima))


def solution(mesh):
    in_specs = (
        P("dp", "tp"),
        P(),
        P(None, "dp", "tp"),
        P(None, "dp", "tp"),
        P(None, "dp", "tp"),
        P(None, "dp", "tp"),
        P(None, "dp", None),
        P(None, "dp", None),
        P(),
        P(None, "dp", "tp"),
        P(None, "dp", "tp", None),
        P(None, "dp", None, None),
        P(None, "dp", None),
    )
    out_specs = (
        P("dp", "tp"),
        P(None, "dp", "tp", None),
        P(None, "dp", None, None),
        P(None, "dp", None),
    )
    return jax.shard_map(shards, mesh=mesh, in_specs=in_specs, out_specs=out_specs, check_vma=False)
```

profile of v0, /device:TPU:0, one launch (start us, length us, event | category | flops | bytes accessed | tf_op | source)
XLA Modules:
  0.0 374.9 jit_solution(8160090856364336624)
XLA Ops:
  13.0 3.1 fusion.172
  21.3 32.4 %all_gather.66 = bf16[8,4096]{1,0:T(8,128)(2,1)S(1)} all-gather(bf16[8,512]{1,0:T(8,128)(2,1)S(1)} %copy-done.7), channel_id=1, replica_groups=mesh['tp'=8,'dp'=4] {'tp'}, dimensions={1}, use_global_device_ids=true | all-gather | bytes 73728 | tf_op jit(solution)/shard_map/all_gather | solution.py:16
  53.9 5.7 %all-gather.2 = bf16[1,4096,16]{1,2,0:T(8,128)(2,1)S(1)} all-gather(bf16[1,1024,16]{1,2,0:T(8,128)(2,1)S(1)} %get-tuple-element.43), channel_id=4, replica_groups=mesh['tp'=8,'dp'=4] {'dp'}, dimensions={1}, use_global_device_ids=true | all-gather | bytes 163840 | tf_op jit(solution)/shard_map/all_gather | solution.py:59
  59.6 5.4 %all-gather.1 = bf16[1,4096,16]{1,2,0:T(8,128)(2,1)S(1)} all-gather(bf16[1,1024,16]{1,2,0:T(8,128)(2,1)S(1)} %get-tuple-element.41), channel_id=3, replica_groups=mesh['tp'=8,'dp'=4] {'dp'}, dimensions={1}, use_global_device_ids=true | all-gather | bytes 163840 | tf_op jit(solution)/shard_map/all_gather | solution.py:60
  67.9 4.3 %fusion.169 = (f32[1,8,512,128]{3,2,1,0:T(8,128)S(1)}, f32[1,8,512,128]{3,2,1,0:T(8,128)}) fusion(f32[2,8,512,128]{3,2,1,0:T(8,128)} %param.27), kind=kLoop, calls=%fused_computation.155 | loop fusion | bytes 8388608 | tf_op jit(solution)/shard_map/slice | solution.py:88
  72.3 6.3 %all-gather.9 = bf16[1,4096,16]{1,2,0:T(8,128)(2,1)S(1)} all-gather(bf16[1,1024,16]{1,2,0:T(8,128)(2,1)S(1)} %get-tuple-element.42), channel_id=11, replica_groups=mesh['tp'=8,'dp'=4] {'dp'}, dimensions={1}, use_global_device_ids=true | all-gather | bytes 163840 | tf_op jit(solution)/shard_map/all_gather | solution.py:59
  78.6 6.3 %all-gather.8 = bf16[1,4096,16]{1,2,0:T(8,128)(2,1)S(1)} all-gather(bf16[1,1024,16]{1,2,0:T(8,128)(2,1)S(1)} %get-tuple-element.40), channel_id=10, replica_groups=mesh['tp'=8,'dp'=4] {'dp'}, dimensions={1}, use_global_device_ids=true | all-gather | bytes 163840 | tf_op jit(solution)/shard_map/all_gather | solution.py:60
  87.1 30.6 %all_gather.72 = bf16[8,2048]{1,0:T(8,128)(2,1)S(1)} all-gather(bf16[8,256]{1,0:T(8,128)(2,1)S(1)} %fusion.104), channel_id=1, replica_groups=mesh['tp'=8,'dp'=4] {'tp'}, dimensions={1}, use_global_device_ids=true | all-gather | bytes 36864 | tf_op jit(solution)/shard_map/all_gather | solution.py:71
  119.7 30.6 %all_gather.74 = bf16[8,2048]{1,0:T(8,128)(2,1)S(1)} all-gather(bf16[8,256]{1,0:T(8,128)(2,1)S(1)} %fusion.107), channel_id=1, replica_groups=mesh['tp'=8,'dp'=4] {'tp'}, dimensions={1}, use_global_device_ids=true | all-gather | bytes 36864 | tf_op jit(solution)/shard_map/all_gather | solution.py:70
  153.2 2.7 gather_fusion.3
  157.2 2.9 fusion.68
  160.3 10.7 %fusion.167 = (f32[1,8,512,128]{3,1,2,0:T(8,128)}, f32[8,512]{0,1:T(8,128)S(1)}) fusion(f32[512,8,128]{2,1,0:T(8,128)} %gather_fusion.2, pred[512]{0:T(512)(128)(4,1)S(1)} %compare_and_fusion, f32[8,512]{0,1:T(8,128)S(1)} %copy.81, f32[1,8,512,128]{3,2,1,0:T(8,128)} %get-tuple-element.27, f32[8,512]{0,1:T(8,128)S(1)} %select_bitcast_fusion.1, ...), kind=kLoop, calls=%fused_computation.153 | loop fusion | flops 3665920 | bytes 8438272 | tf_op jit(solution)/shard_map/stack | solution.py:103
  171.0 2.9 fusion.59
  173.9 30.5 %all_gather.75 = bf16[8,4096]{1,0:T(8,128)(2,1)S(1)} all-gather(bf16[8,512]{1,0:T(8,128)(2,1)S(1)} %fusion.59), channel_id=1, replica_groups=mesh['tp'=8,'dp'=4] {'tp'}, dimensions={1}, use_global_device_ids=true | all-gather | bytes 73728 | tf_op jit(solution)/shard_map/all_gather | solution.py:16
  204.5 2.9 fusion.35
  207.3 30.5 %all_gather.77 = bf16[8,4096]{1,0:T(8,128)(2,1)S(1)} all-gather(bf16[8,512]{1,0:T(8,128)(2,1)S(1)} %fusion.35), channel_id=1, replica_groups=mesh['tp'=8,'dp'=4] {'tp'}, dimensions={1}, use_global_device_ids=true | all-gather | bytes 73728 | tf_op jit(solution)/shard_map/all_gather | solution.py:16
  241.7 30.6 %all_gather.83 = bf16[8,2048]{1,0:T(8,128)(2,1)S(1)} all-gather(bf16[8,256]{1,0:T(8,128)(2,1)S(1)} %fusion.110), channel_id=1, replica_groups=mesh['tp'=8,'dp'=4] {'tp'}, dimensions={1}, use_global_device_ids=true | all-gather | bytes 36864 | tf_op jit(solution)/shard_map/all_gather | solution.py:71
  274.4 2.9 fusion.101
  279.5 30.8 %all_gather.85 = bf16[8,2048]{1,0:T(8,128)(2,1)S(1)} all-gather(bf16[8,256]{1,0:T(8,128)(2,1)S(1)} %fusion.113), channel_id=1, replica_groups=mesh['tp'=8,'dp'=4] {'tp'}, dimensions={1}, use_global_device_ids=true | all-gather | bytes 36864 | tf_op jit(solution)/shard_map/all_gather | solution.py:70
  316.1 10.1 %fusion.168 = (f32[1,8,512,128]{3,1,2,0:T(8,128)S(1)}, f32[8,512]{0,1:T(8,128)S(1)}) fusion(f32[512,8,128]{2,1,0:T(8,128)} %gather_fusion.7, pred[512]{0:T(512)(128)(4,1)S(1)} %compare_and_fusion, f32[8,512]{0,1:T(8,128)S(1)} %copy.91, f32[1,8,512,128]{3,2,1,0:T(8,128)S(1)} %get-tuple-element.26, f32[8,512]{0,1:T(8,128)S(1)} %select_bitcast_fusion, ...), kind=kLoop, calls=%fused_computation.154 | loop fusion | flops 3665920 | bytes 8438272 | tf_op jit(solution)/shard_map/stack | solution.py:103
  326.5 2.8 copy.101
  330.6 2.9 fusion.92
  333.5 30.5 %all_gather.86 = bf16[8,4096]{1,0:T(8,128)(2,1)S(1)} all-gather(bf16[8,512]{1,0:T(8,128)(2,1)S(1)} %fusion.92), channel_id=1, replica_groups=mesh['tp'=8,'dp'=4] {'tp'}, dimensions={1}, use_global_device_ids=true | all-gather | bytes 73728 | tf_op jit(solution)/shard_map/all_gather | solution.py:16
  364.6 3.4 fusion.32
  (113 shorter events, 38.3 us)
Async XLA Ops:
  7.2 2.4 copy-start.3
  7.2 77.8 %all-gather.29.cloned.1.call-start = ((), (), s32[]{:S(2)}) async-start(), calls=%async_computation.2 | async-start | bytes 2621440 | tf_op jit(solution)/shard_map/all_gather | solution.py:56
  9.5 2.0 copy-start.1
  9.6 108.1 %all-gather.31.cloned.1.call-start = ((), (), s32[]{:S(2)}) async-start(), calls=%async_computation.3 | async-start | bytes 2621440 | tf_op jit(solution)/shard_map/all_gather | solution.py:55
  10.7 146.5 %all-gather.27.cloned.1.call-start = ((), (), s32[]{:S(2)}) async-start(), calls=%async_computation.1 | async-start | bytes 5242880 | tf_op jit(solution)/shard_map/all_gather | solution.py:57
  13.0 3.3 copy-start.2
  13.0 158.1 %all-gather.25.cloned.1.call-start = ((), (), s32[]{:S(2)}) async-start(), calls=%async_computation | async-start | bytes 5242880 | tf_op jit(solution)/shard_map/all_gather | solution.py:58
  16.2 188.3 %all-gather.33.cloned.1.call-start = ((), (), s32[]{:S(2)}) async-start(), calls=%async_computation.4 | async-start | bytes 5242880 | tf_op jit(solution)/shard_map/all_gather | solution.py:96
  17.9 221.9 %all-gather.39.cloned.1.call-start = ((), (), s32[]{:S(2)}) async-start(), calls=%async_computation.7 | async-start | bytes 2621440 | tf_op jit(solution)/shard_map/all_gather | solution.py:56
  17.9 3.4 copy-start.7
  17.9 35.9 %copy-start.8 = (f32[2,4096]{1,0:T(2,128)S(1)}, f32[2,4096]{1,0:T(2,128)}, u32[]{:S(2)}) copy-start(f32[2,4096]{1,0:T(2,128)} %param.18) | copy-start | bytes 98308
  17.9 36.0 %copy-start.5 = (bf16[2,1024,16]{1,2,0:T(8,128)(2,1)S(1)}, bf16[2,1024,16]{1,2,0:T(8,128)(2,1)}, u32[]{:S(2)}) copy-start(bf16[2,1024,16]{1,2,0:T(8,128)(2,1)} %param.23) | copy-start | bytes 196612
  18.4 255.9 %all-gather.37.cloned.1.call-start = ((), (), s32[]{:S(2)}) async-start(), calls=%async_computation.6 | async-start | bytes 5242880 | tf_op jit(solution)/shard_map/all_gather | solution.py:57
  18.5 41.1 %copy-start.6 = (bf16[2,1024,16]{1,2,0:T(8,128)(2,1)S(1)}, bf16[2,1024,16]{1,2,0:T(8,128)(2,1)}, u32[]{:S(2)}) copy-start(bf16[2,1024,16]{1,2,0:T(8,128)(2,1)} %param.24) | copy-start | bytes 196612
  18.5 46.5 %copy-start.10 = (f32[2,16]{1,0:T(2,128)S(1)}, f32[2,16]{1,0:T(2,128)}, u32[]{:S(2)}) copy-start(f32[2,16]{1,0:T(2,128)} %param.25) | copy-start | bytes 388
  19.2 46.0 %copy-start.9 = (f32[2,8,16]{2,1,0:T(8,128)S(1)}, f32[2,8,16]{2,1,0:T(8,128)}, u32[]{:S(2)}) copy-start(f32[2,8,16]{2,1,0:T(8,128)} %param.29) | copy-start | bytes 3076
  19.2 46.4 %copy-start.4 = (f32[2,8,16,128]{3,2,1,0:T(8,128)S(1)}, f32[2,8,16,128]{3,2,1,0:T(8,128)}, u32[]{:S(2)}) copy-start(f32[2,8,16,128]{3,2,1,0:T(8,128)} %param.28) | copy-start | bytes 393220
  19.2 258.2 %all-gather.41.cloned.1.call-start = ((), (), s32[]{:S(2)}) async-start(), calls=%async_computation.8 | async-start | bytes 2621440 | tf_op jit(solution)/shard_map/all_gather | solution.py:55
  20.0 310.6 %all-gather.35.cloned.1.call-start = ((), (), s32[]{:S(2)}) async-start(), calls=%async_computation.5 | async-start | bytes 5242880 | tf_op jit(solution)/shard_map/all_gather | solution.py:58
  20.7 343.9 %all-gather.43.cloned.1.call-start = ((), (), s32[]{:S(2)}) async-start(), calls=%async_computation.9 | async-start | bytes 5242880 | tf_op jit(solution)/shard_map/all_gather | solution.py:96
  316.1 10.1 %copy-start = (f32[1,8,512,128]{3,1,2,0:T(8,128)S(1)}, f32[1,8,512,128]{3,1,2,0:T(8,128)}, u32[]{:S(2)}) copy-start(f32[1,8,512,128]{3,1,2,0:T(8,128)} %get-tuple-element.22) | copy-start | bytes 6291460
Sparse Core Ops, SparseCore 0:
  10.1 25.2 all-gather.28
  37.0 23.0 all-gather.30
  61.7 35.8 all-gather.26
  99.0 34.4 all-gather.24
  134.9 34.4 all-gather.32
  170.8 22.5 all-gather.38
  195.0 34.4 all-gather.36
  231.0 22.5 all-gather.40
  255.2 34.4 all-gather.34
  291.1 34.4 all-gather.42
where the time goes:
time: 376 us; the launch traced here: 375 us
  blocking collectives  270 us (72%)
  local copies, waits for them, and re-layouts  36.6 us (10%)
  matrix products  27 us (7%)
  other arithmetic  22.9 us (6%)
  between operations  14.6 us (4%)
    all_gather x4, blocking collectives, full_rows(): return lax.all_gather(shard, 'tp', axis=1, tiled=True)  124 us
    all_gather x2, blocking collectives, shards(): lax.all_gather(query, 'tp', axis=1, tiled=True)  61.4 us
    all_gather x2, blocking collectives, shards(): lax.all_gather(keys, 'tp', axis=1, tiled=True)  61.2 us
    another operation x3, other arithmetic, shards(): jnp.stack(memories)  21.1 us
    dot_general x12, matrix products, fold_with(): jnp.dot(activations, piece, preferred_element_type=jnp.float32)  20.7 us
    all_gather x2, blocking collectives, shards(): lax.all_gather(w_ingate[layer], 'dp', axis=0, tiled=True)  12 us
    all_gather x2, blocking collectives, shards(): lax.all_gather(w_forget[layer], 'dp', axis=0, tiled=True)  11.7 us
  transfers between devices with their start and end apart: 10, of which 0 were waited for; matrix products, arithmetic and copies ran while one was open for 21% of the time, Pallas kernels for 0%

commit v1 on v0

--- a/solution.py
+++ b/solution.py
@@ -1,6 +1,10 @@
+import functools
+
 import jax
 import jax.numpy as jnp
 from jax import lax
+from jax.experimental import pallas as pl
+from jax.experimental.pallas import tpu as pltpu
 from jax.sharding import PartitionSpec as P
 
 H = 16
@@ -22,7 +26,7 @@
     )
 
 
-def shards(
+def gathered(
     tokens,
     norm_gain,
     w_query,
@@ -103,6 +107,304 @@
     return (current, jnp.stack(memories), jnp.stack(normalisers), jnp.stack(maxima))
 
 
+WIRE = jnp.bfloat16
+MESH = pl.DeviceIdType.MESH
+
+
+def fused_kernel(
+    tp, dp,
+    tokens, gain, w_query, w_key, w_value, w_outgate, w_in, w_fg, bias, w_output, mem, norm, peak,
+    mixed, mem_out, norm_out, peak_out,
+    wq, wk, wv, wo, wi, wf, wp, state,
+    cur, xg, gs, cg, part, got, gate_part, gate_got, up_part, up_got, nn,
+    load_sem, out_sem, xs_sem, xr_sem, gs_sem, gr_sem, ps_sem, pr_sem, us_sem, ur_sem, ns_sem, nr_sem,
+):
+    t, d = lax.axis_index("tp"), lax.axis_index("dp")
+    seqs, feats = tokens.shape
+    rows = wq.shape[1]
+    qcols, vcols = wq.shape[2], wv.shape[2]
+    group = rows // feats
+    own_heads = vcols // DV
+    features = gain.shape[1]
+    heads = peak.shape[2]
+    f32, bf16 = jnp.float32, jnp.bfloat16
+
+    loads = {}
+    order = ((w_in, wi), (w_fg, wf), (w_query, wq), (w_key, wk), (w_value, wv), (w_outgate, wo), (mem, state), (w_output, wp))
+    for b in range(BLOCKS):
+        for i, (src, dst) in enumerate(order):
+            c = pltpu.make_async_copy(src.at[b], dst.at[b], load_sem.at[b, i])
+            c.start()
+            loads[b, i] = c
+
+    sends = []
+
+    def spread(src, dst, send_sem, recv_sem):
+        home, slot = t // group, t % group
+        here = home == d
+
+        def to(target, k):
+            return pltpu.make_async_remote_copy(
+                src_ref=src, dst_ref=dst.at[d, slot], send_sem=send_sem.at[k], recv_sem=recv_sem.at[d, slot],
+                device_id={"tp": target, "dp": home}, device_id_type=MESH,
+            )
+
+        for k in range(tp - 1, 0, -1):
+            c = to((t + k) % tp, k)
+            c.start()
+            sends.append((None, c))
+
+        @pl.when(jnp.logical_not(here))
+        def _():
+            to(t, 0).start()
+
+        @pl.when(here)
+        def _():
+            dst[d, slot] = src[...]
+
+        sends.append((jnp.logical_not(here), to(t, 0)))
+
+    def collect(dst, send_sem, recv_sem, dd, g):
+        @pl.when(jnp.logical_or(d * group + g != t, d != dd))
+        def _():
+            pltpu.make_async_remote_copy(
+                src_ref=dst.at[dd, g], dst_ref=dst.at[dd, g], send_sem=send_sem.at[0], recv_sem=recv_sem.at[dd, g],
+                device_id={"tp": (t + 1) % tp, "dp": d}, device_id_type=MESH,
+            ).wait_recv()
+
+    def to_owners(src, dst, send_sem, recv_sem, view):
+        copies = []
+        for k in range(1, dp):
+            dd = (d + k) % dp
+            c = pltpu.make_async_remote_copy(
+                src_ref=src.at[(dd,) + view], dst_ref=dst.at[(k - 1,) + view],
+                send_sem=send_sem.at[k - 1], recv_sem=recv_sem.at[k - 1],
+                device_id={"tp": t, "dp": dd}, device_id_type=MESH,
+            )
+            c.start()
+            copies.append(c)
+            sends.append((None, c))
+        return copies
+
+    def total(src, dst, view, copies):
+        acc = src[(d,) + view].astype(f32)
+        for k in range(dp - 1):
+            copies[k].wait_recv()
+            acc = acc + dst[(k,) + view].astype(f32)
+        return acc
+
+    gate_part[...] = jnp.zeros_like(gate_part)
+    norms = []
+    lane = lax.broadcasted_iota(jnp.int32, (seqs, heads), 1)
+    row = lax.broadcasted_iota(jnp.int32, (seqs, DV), 0)
+    everything = (slice(None), slice(None), slice(None))
+
+    for b in range(BLOCKS):
+        here = tokens if b == 0 else cur.at[b]
+        spread(here, xg.at[b], xs_sem.at[b], xr_sem.at[b])
+        for dd in range(dp):
+            for g in range(group):
+                collect(xg.at[b], xs_sem.at[b], xr_sem.at[b], dd, g)
+        pieces = []
+        square = jnp.zeros((dp * seqs, 1), f32)
+        for g in range(group):
+            wide = jnp.concatenate([xg[b, dd, g].astype(f32) for dd in range(dp)], axis=0)
+            square = square + jnp.sum(wide * wide, axis=1, keepdims=True)
+            at = pl.multiple_of(d * rows + g * feats, feats)
+            pieces.append((wide * gain[b : b + 1, pl.ds(at, feats)]).astype(bf16))
+        x = jnp.concatenate(pieces, axis=1)
+
+        loads[b, 0].wait()
+        loads[b, 1].wait()
+        pre = (jnp.dot(x, wi[b], preferred_element_type=f32), jnp.dot(x, wf[b], preferred_element_type=f32))
+        for dd in range(dp):
+            own = slice(dd * seqs, (dd + 1) * seqs)
+            gate_part[b, dd, 0, :, 0:heads] = pre[0][own]
+            gate_part[b, dd, 1, :, 0:heads] = pre[1][own]
+            gate_part[b, dd, 2] = jnp.broadcast_to(square[own], (seqs, gate_part.shape[-1]))
+        gate_copies = to_owners(gate_part.at[b], gate_got.at[b], ps_sem.at[b, 0], pr_sem.at[b, 0], everything)
+
+        spans, flights, at = [], [], 0
+        for chunk, members in enumerate((((2, wq), (3, wk)), ((4, wv),), ((5, wo),))):
+            begin = at
+            for i, w in members:
+                loads[b, i].wait()
+                p = jnp.dot(x, w[b], preferred_element_type=f32).astype(WIRE)
+                n = w.shape[2]
+                for dd in range(dp):
+                    part[b, dd, :, at : at + n] = p[dd * seqs : (dd + 1) * seqs]
+                at += n
+            view = (slice(None), pl.ds(begin, at - begin))
+            spans.append(view)
+            flights.append(to_owners(part.at[b], got.at[b], ps_sem.at[b, chunk + 1], pr_sem.at[b, chunk + 1], view))
+
+        gates = total(gate_part.at[b], gate_got.at[b], everything, gate_copies)
+        scale = lax.rsqrt(gates[2][:, 0:1] * (1.0 / features) + EPSILON)
+        in_pre = gates[0][:, :heads] * scale
+        forget = gates[1][:, :heads] * scale + bias[b : b + 1, :]
+        log_forget = jnp.minimum(forget, 0.0) - jnp.log1p(jnp.exp(-jnp.abs(forget)))
+        moved = log_forget + peak[b]
+        new_peak = jnp.maximum(moved, in_pre)
+        carried = jnp.exp(moved - new_peak)
+        fresh = jnp.exp(in_pre - new_peak)
+        peak_out[b] = new_peak
+
+        qk = (total(part.at[b], got.at[b], spans[0], flights[0]) * scale).astype(bf16).astype(f32)
+        loads[b, 6].wait()
+        stage = []
+        for hh in range(own_heads):
+            mine = lane == t * own_heads + hh
+            c_h = jnp.sum(jnp.where(mine, carried, 0.0), axis=1, keepdims=True)
+            f_h = jnp.sum(jnp.where(mine, fresh, 0.0), axis=1, keepdims=True)
+            q_h = qk[:, hh * DK : (hh + 1) * DK]
+            k_h = qk[:, qcols + hh * DK : qcols + (hh + 1) * DK] * DK ** (-0.5)
+            n_h = c_h * norm[b, :, t * own_heads + hh, :] + f_h * k_h
+            nn[b, t, hh] = n_h
+            div = jnp.maximum(jnp.abs(jnp.sum(n_h * q_h, axis=1, keepdims=True)), 1.0)
+            kq = jnp.sum(k_h * q_h, axis=1, keepdims=True)
+            q_b = q_h.astype(bf16)
+            read = jnp.zeros((seqs, DV), f32)
+            for s in range(seqs):
+                c = state[b, s, hh * DV : (hh + 1) * DV, :].astype(bf16)
+                r = lax.dot_general(q_b, c, (((1,), (1,)), ((), ())), preferred_element_type=f32)
+                read = read + jnp.where(row == s, r, 0.0)
+            stage.append((c_h, f_h, k_h, div, kq, read))
+
+        v = (total(part.at[b], got.at[b], spans[1], flights[1]) * scale).astype(bf16).astype(f32)
+        o = (total(part.at[b], got.at[b], spans[2], flights[2]) * scale).astype(bf16).astype(f32)
+        for hh, (c_h, f_h, k_h, div, kq, read) in enumerate(stage):
+            cols = slice(hh * DV, (hh + 1) * DV)
+            readout = (c_h * read + (f_h * kq) * v[:, cols]) / div
+            gs[b, :, cols] = (jax.nn.sigmoid(o[:, cols]) * readout).astype(bf16)
+        spread(gs.at[b], cg.at[b], gs_sem.at[b], gr_sem.at[b])
+
+        for k in range(1, tp):
+            c = pltpu.make_async_remote_copy(
+                src_ref=nn.at[b, t], dst_ref=nn.at[b, t], send_sem=ns_sem.at[b, k - 1], recv_sem=nr_sem.at[b, k - 1],
+                device_id={"tp": (t + k) % tp, "dp": d}, device_id_type=MESH,
+            )
+            c.start()
+            sends.append((None, c))
+            norms.append((k, b))
+
+        for hh, (c_h, f_h, k_h, div, kq, read) in enumerate(stage):
+            cols = slice(hh * DV, (hh + 1) * DV)
+            v_t = jnp.transpose(v[:, cols] * f_h)
+            for s in range(seqs):
+                state[b, s, cols, :] = c_h[s : s + 1] * state[b, s, cols, :] + v_t[:, s : s + 1] * k_h[s : s + 1]
+        store = pltpu.make_async_copy(state.at[b], mem_out.at[b], out_sem.at[b])
+        store.start()
+        loads[b, "store"] = store
+
+        for dd in range(dp):
+            for g in range(group):
+                collect(cg.at[b], gs_sem.at[b], gr_sem.at[b], dd, g)
+        gated = jnp.concatenate(
+            [
+                jnp.concatenate([cg[b, dd, g].astype(f32) for dd in range(dp)], axis=0).astype(bf16)
+                for g in range(group)
+            ],
+            axis=1,
+        )
+        loads[b, 7].wait()
+        up = jnp.dot(gated, wp[b], preferred_element_type=f32)
+        for dd in range(dp):
+            up_part[b, dd] = up[dd * seqs : (dd + 1) * seqs]
+        flat = (slice(None), slice(None))
+        copies = to_owners(up_part.at[b], up_got.at[b], us_sem.at[b], ur_sem.at[b], flat)
+        update = total(up_part.at[b], up_got.at[b], flat, copies)
+        after = (here[...].astype(f32) + update).astype(bf16)
+        if b + 1 < BLOCKS:
+            cur[b + 1] = after
+        else:
+            mixed[...] = after
+
+    for k, b in norms:
+        pltpu.make_async_remote_copy(
+            src_ref=nn.at[b, t], dst_ref=nn.at[b, (t + tp - k) % tp], send_sem=ns_sem.at[b, k - 1],
+            recv_sem=nr_sem.at[b, k - 1], device_id={"tp": (t + k) % tp, "dp": d}, device_id_type=MESH,
+        ).wait_recv()
+    for b in range(BLOCKS):
+        for i in range(tp):
+            for hh in range(own_heads):
+                norm_out[b, i * own_heads + hh] = nn[b, i, hh]
+        loads[b, "store"].wait()
+    for cond, c in sends:
+        if cond is None:
+            c.wait_send()
+        else:
+            pl.when(cond)(c.wait_send)
+
+
+def fused(tp, dp, tokens, gain, w_query, w_key, w_value, w_outgate, w_in, w_fg, bias, w_output, mem, norm, peak):
+    seqs, feats = tokens.shape
+    rows, vcols = w_value.shape[1:]
+    group, own_heads = rows // feats, vcols // DV
+    heads = peak.shape[2]
+    width = 2 * w_query.shape[2] + 2 * vcols
+    anywhere, vmem = pl.BlockSpec(memory_space=pl.ANY), pl.BlockSpec(memory_space=pltpu.VMEM)
+    f32, bf16 = jnp.float32, jnp.bfloat16
+    dma = pltpu.SemaphoreType.DMA
+    big = (w_query, w_key, w_value, w_outgate, w_in, w_fg, w_output, mem)
+    others = max(dp - 1, 1)
+    mixed, new_mem, new_norm, new_peak = pl.pallas_call(
+        functools.partial(fused_kernel, tp, dp),
+        out_shape=(
+            jax.ShapeDtypeStruct(tokens.shape, tokens.dtype),
+            jax.ShapeDtypeStruct(mem.shape, mem.dtype),
+            jax.ShapeDtypeStruct((BLOCKS, heads, seqs, DK), f32),
+            jax.ShapeDtypeStruct(peak.shape, f32),
+        ),
+        in_specs=[vmem, vmem] + [anywhere] * 6 + [vmem, anywhere, anywhere, vmem, vmem],
+        out_specs=(vmem, anywhere, vmem, vmem),
+        scratch_shapes=[pltpu.VMEM(w.shape, w.dtype) for w in big]
+        + [
+            pltpu.VMEM((BLOCKS, seqs, feats), bf16),
+            pltpu.VMEM((BLOCKS, dp, group, seqs, feats), bf16),
+            pltpu.VMEM((BLOCKS, seqs, vcols), bf16),
+            pltpu.VMEM((BLOCKS, dp, group, seqs, vcols), bf16),
+            pltpu.VMEM((BLOCKS, dp, seqs, width), WIRE),
+            pltpu.VMEM((BLOCKS, others, seqs, width), WIRE),
+            pltpu.VMEM((BLOCKS, dp, 3, seqs, 128), f32),
+            pltpu.VMEM((BLOCKS, others, 3, seqs, 128), f32),
+            pltpu.VMEM((BLOCKS, dp, seqs, feats), f32),
+            pltpu.VMEM((BLOCKS, others, seqs, feats), f32),
+            pltpu.VMEM((BLOCKS, tp, own_heads, seqs, DK), f32),
+            dma((BLOCKS, 8)),
+            dma((BLOCKS,)),
+            dma((BLOCKS, tp)),
+            dma((BLOCKS, dp, group)),
+            dma((BLOCKS, tp)),
+            dma((BLOCKS, dp, group)),
+            dma((BLOCKS, 4, others)),
+            dma((BLOCKS, 4, others)),
+            dma((BLOCKS, others)),
+            dma((BLOCKS, others)),
+            dma((BLOCKS, tp)),
+            dma((BLOCKS, tp)),
+        ],
+        compiler_params=pltpu.CompilerParams(has_side_effects=True, vmem_limit_bytes=60 * 1024 * 1024),
+    )(tokens, gain, w_query, w_key, w_value, w_outgate, w_in, w_fg, bias, w_output, mem, norm, peak)
+    return mixed, new_mem, jnp.transpose(new_norm, (0, 2, 1, 3)), new_peak
+
+
+def whole_heads(tp, dp, *args):
+    tokens, w_query, w_value, w_output = args[0], args[2], args[4], args[9]
+    seqs, feats = tokens.shape
+    rows, vcols = w_value.shape[1:]
+    return (
+        tp > 1 and dp > 1 and seqs % 8 == 0 and feats % 128 == 0
+        and vcols % DV == 0 and w_query.shape[2] == vcols // DV * DK
+        and rows % feats == 0 and vcols == feats and w_output.shape[1] == rows
+    )
+
+
+def shards(tp, dp, *args):
+    if whole_heads(tp, dp, *args):
+        return fused(tp, dp, *args)
+    return gathered(*args)
+
+
 def solution(mesh):
     in_specs = (
         P("dp", "tp"),
@@ -125,4 +427,5 @@
         P(None, "dp", None, None),
         P(None, "dp", None),
     )
-    return jax.shard_map(shards, mesh=mesh, in_specs=in_specs, out_specs=out_specs, check_vma=False)
+    body = functools.partial(shards, mesh.shape["tp"], mesh.shape["dp"])
+    return jax.shard_map(body, mesh=mesh, in_specs=in_specs, out_specs=out_specs, check_vma=False)

time: 376 us -> 55.7 us (0.15)
  blocking collectives: 270 us -> 0 us
  Pallas kernels: 0 us -> 43 us
  matrix products: 27 us -> 0 us
  local copies, waits for them, and re-layouts: 36.6 us -> 11.8 us
  other arithmetic: 22.9 us -> 0 us
  between operations: 14.6 us -> 0.64 us
    all_gather x12 -> x0, blocking collectives: 270 us -> none  [the longest x4 124 us: full_rows(): return lax.all_gather(shard, 'tp', axis=1, tiled=True)]
    pallas_call x0 -> x1, Pallas kernels: none -> 43 us  [fused(): pl.pallas_call(functools.partial(fused_kernel, tp, dp), out_shape=(jax.Sh...]
    dot_general x14 -> x0, matrix products: 27 us -> none  [the longest x12 20.7 us: fold_with(): jnp.dot(activations, piece, preferred_element_type=jnp.float32)]
    another operation x5 -> x0, other arithmetic: 21.7 us -> none  [the longest x3 21.1 us: shards(): jnp.stack(memories)]
    gather x14 -> x0, local copies, waits for them, and re-layouts: 17.5 us -> none  [the longest x2 5.49 us: shards(): query_cols = jnp.take(query_heads, column_head, axis=1)]
    slice x10 -> x0, local copies, waits for them, and re-layouts: 13.9 us -> none  [the longest x1 4.34 us: shards(): mem_state[layer]]
    unnamed x24 -> x8, local copies, waits for them, and re-layouts: 4.31 us -> 11.8 us
  transfers between devices with their start and end apart: 10 -> 0, of which waited for: 0 -> 0; matrix products, arithmetic and copies ran while one was open for 21% -> 0% of each run, Pallas kernels for 0% -> 0%
where the time goes in v1:
time: 55.7 us; the launch traced here: 55.4 us
  Pallas kernels  43 us (77%)
  local copies, waits for them, and re-layouts  11.8 us (21%)
  between operations  0.64 us (1%)
    pallas_call x1, Pallas kernels, fused(): pl.pallas_call(functools.partial(fused_kernel, tp, dp), out_shape=(jax.Sh...  43 us
    unnamed x8, local copies, waits for them, and re-layouts  11.8 us

profile of v1, /device:TPU:0, one launch (start us, length us, event | category | flops | bytes accessed | tf_op | source)
XLA Modules:
  0.0 55.4 jit_solution(13854695247670942947)
XLA Ops:
  0.6 1.8 %copy.17.w_in = bf16[2,1024,16]{2,1,0:T(8,128)(2,1)} copy(bf16[2,1024,16]{1,2,0:T(8,128)(2,1)} %param.19) | data formatting | bytes 131072 | tf_op args[6]
  2.5 1.8 %copy.18.w_fg = bf16[2,1024,16]{2,1,0:T(8,128)(2,1)} copy(bf16[2,1024,16]{1,2,0:T(8,128)(2,1)} %param.20) | data formatting | bytes 131072 | tf_op args[7]
  4.3 43.0 %shard_map.156 = (bf16[8,512]{1,0:T(8,128)(2,1)}, f32[2,8,512,128]{3,2,1,0:T(8,128)}, f32[2,16,8,128]{3,2,1,0:T(8,128)}, f32[2,8,16]{2,1,0:T(8,128)}) custom-call(bf16[8,512]{1,0:T(8,128)(2,1)} %tokens.1, f32[2,4096]{1,0:T(2,128)} %gain.1, bf16[2,1024,256]{2,1,0:T(8,128)(2,1)} %w_query.1, bf16[2,1024,256]{2,1,0:T(8,128)(2,1)} %w_key.1, ...), custom_call_target="tpu_custom_call" | custom-call | tf_op jit(solution)/shard_map/pallas_call | solution.py:350
  47.3 1.6 %copy.19 = f32[2,8,16,128]{3,2,1,0:T(8,128)} copy(f32[2,8,16,128]{3,1,2,0:T(8,128)} %bitcast.1) | data formatting | bytes 262144
  48.9 1.3 %copy.23 = bf16[8,512]{1,0:T(8,128)(2,1)} copy(bf16[8,512]{1,0:T(8,128)(2,1)} %get-tuple-element.20) | data formatting | bytes 16384
  50.2 0.0 copy-start
  50.2 4.6 %copy.24 = f32[2,8,512,128]{3,2,1,0:T(8,128)} copy(f32[2,8,512,128]{3,2,1,0:T(8,128)} %get-tuple-element.21) | data formatting | bytes 8388608
  54.8 0.0 copy-done
  54.8 0.6 %copy.25 = f32[2,8,16]{2,1,0:T(8,128)} copy(f32[2,8,16]{2,1,0:T(8,128)S(1)} %copy-done) | data formatting | bytes 2048
Async XLA Ops:
  50.2 4.6 %copy-start = (f32[2,8,16]{2,1,0:T(8,128)S(1)}, f32[2,8,16]{2,1,0:T(8,128)}, u32[]{:S(2)}) copy-start(f32[2,8,16]{2,1,0:T(8,128)} %get-tuple-element.23) | copy-start | bytes 3076

commit v2 on v1

--- a/solution.py
+++ b/solution.py
@@ -113,11 +113,11 @@
 
 def fused_kernel(
     tp, dp,
-    tokens, gain, w_query, w_key, w_value, w_outgate, w_in, w_fg, bias, w_output, mem, norm, peak,
-    mixed, mem_out, norm_out, peak_out,
-    wq, wk, wv, wo, wi, wf, wp, state,
+    tokens, gain_in, w_query, w_key, w_value, w_outgate, w_in, w_fg, bias_in, w_output, mem, norm_in, peak_in,
+    mixed, state, norm_out, peak_out,
+    wq, wk, wv, wo, wi, wp, gain, bias, norm, peak,
     cur, xg, gs, cg, part, got, gate_part, gate_got, up_part, up_got, nn,
-    load_sem, out_sem, xs_sem, xr_sem, gs_sem, gr_sem, ps_sem, pr_sem, us_sem, ur_sem, ns_sem, nr_sem,
+    small_sem, load_sem, xs_sem, xr_sem, gs_sem, gr_sem, ps_sem, pr_sem, us_sem, ur_sem, ns_sem, nr_sem,
 ):
     t, d = lax.axis_index("tp"), lax.axis_index("dp")
     seqs, feats = tokens.shape
@@ -129,13 +129,32 @@
     heads = peak.shape[2]
     f32, bf16 = jnp.float32, jnp.bfloat16
 
+    smalls = []
+    for i, (src, dst) in enumerate(
+        ((tokens, cur.at[0]), (gain_in, gain), (bias_in, bias), (norm_in, norm), (peak_in, peak))
+    ):
+        c = pltpu.make_async_copy(src, dst, small_sem.at[i])
+        c.start()
+        smalls.append(c)
     loads = {}
-    order = ((w_in, wi), (w_fg, wf), (w_query, wq), (w_key, wk), (w_value, wv), (w_outgate, wo), (mem, state), (w_output, wp))
+    order = ((w_in, wi), (w_fg, wi), (w_query, wq), (w_key, wk), (w_value, wv), (w_outgate, wo), (mem, state), (w_output, wp))
     for b in range(BLOCKS):
         for i, (src, dst) in enumerate(order):
-            c = pltpu.make_async_copy(src.at[b], dst.at[b], load_sem.at[b, i])
+            to = dst.at[b, pl.ds(i * heads, heads)] if i < 2 else dst.at[b]
+            c = pltpu.make_async_copy(src.at[b], to, load_sem.at[b, i])
             c.start()
             loads[b, i] = c
+
+    barrier = pltpu.get_barrier_semaphore()
+    for i in range(tp):
+        for j in range(dp):
+            if i + j > 0:
+                there = {"tp": (t + i) % tp, "dp": (d + j) % dp}
+                pl.semaphore_signal(barrier, inc=1, device_id=there, device_id_type=MESH)
+    gate_part[...] = jnp.zeros_like(gate_part)
+    for c in smalls:
+        c.wait()
+    pl.semaphore_wait(barrier, tp * dp - 1)
 
     sends = []
 
@@ -193,14 +212,13 @@
             acc = acc + dst[(k,) + view].astype(f32)
         return acc
 
-    gate_part[...] = jnp.zeros_like(gate_part)
     norms = []
     lane = lax.broadcasted_iota(jnp.int32, (seqs, heads), 1)
     row = lax.broadcasted_iota(jnp.int32, (seqs, DV), 0)
-    everything = (slice(None), slice(None), slice(None))
+    everything = (slice(None), slice(None))
 
     for b in range(BLOCKS):
-        here = tokens if b == 0 else cur.at[b]
+        here = cur.at[b]
         spread(here, xg.at[b], xs_sem.at[b], xr_sem.at[b])
         for dd in range(dp):
             for g in range(group):
@@ -216,12 +234,11 @@
 
         loads[b, 0].wait()
         loads[b, 1].wait()
-        pre = (jnp.dot(x, wi[b], preferred_element_type=f32), jnp.dot(x, wf[b], preferred_element_type=f32))
+        pre = lax.dot_general(x, wi[b], (((1,), (1,)), ((), ())), preferred_element_type=f32)
         for dd in range(dp):
             own = slice(dd * seqs, (dd + 1) * seqs)
-            gate_part[b, dd, 0, :, 0:heads] = pre[0][own]
-            gate_part[b, dd, 1, :, 0:heads] = pre[1][own]
-            gate_part[b, dd, 2] = jnp.broadcast_to(square[own], (seqs, gate_part.shape[-1]))
+            gate_part[b, dd, :, 0 : 2 * heads] = pre[own]
+            gate_part[b, dd, :, 2 * heads : 2 * heads + 1] = square[own]
         gate_copies = to_owners(gate_part.at[b], gate_got.at[b], ps_sem.at[b, 0], pr_sem.at[b, 0], everything)
 
         spans, flights, at = [], [], 0
@@ -239,9 +256,9 @@
             flights.append(to_owners(part.at[b], got.at[b], ps_sem.at[b, chunk + 1], pr_sem.at[b, chunk + 1], view))
 
         gates = total(gate_part.at[b], gate_got.at[b], everything, gate_copies)
-        scale = lax.rsqrt(gates[2][:, 0:1] * (1.0 / features) + EPSILON)
-        in_pre = gates[0][:, :heads] * scale
-        forget = gates[1][:, :heads] * scale + bias[b : b + 1, :]
+        scale = lax.rsqrt(gates[:, 2 * heads : 2 * heads + 1] * (1.0 / features) + EPSILON)
+        in_pre = gates[:, :heads] * scale
+        forget = gates[:, heads : 2 * heads] * scale + bias[b : b + 1, :]
         log_forget = jnp.minimum(forget, 0.0) - jnp.log1p(jnp.exp(-jnp.abs(forget)))
         moved = log_forget + peak[b]
         new_peak = jnp.maximum(moved, in_pre)
@@ -292,10 +309,6 @@
             v_t = jnp.transpose(v[:, cols] * f_h)
             for s in range(seqs):
                 state[b, s, cols, :] = c_h[s : s + 1] * state[b, s, cols, :] + v_t[:, s : s + 1] * k_h[s : s + 1]
-        store = pltpu.make_async_copy(state.at[b], mem_out.at[b], out_sem.at[b])
-        store.start()
-        loads[b, "store"] = store
-
         for dd in range(dp):
             for g in range(group):
                 collect(cg.at[b], gs_sem.at[b], gr_sem.at[b], dd, g)
@@ -327,13 +340,33 @@
     for b in range(BLOCKS):
         for i in range(tp):
             for hh in range(own_heads):
-                norm_out[b, i * own_heads + hh] = nn[b, i, hh]
-        loads[b, "store"].wait()
+                norm_out[b, :, i * own_heads + hh, :] = nn[b, i, hh]
     for cond, c in sends:
         if cond is None:
             c.wait_send()
         else:
             pl.when(cond)(c.wait_send)
+
+
+def write_kernel(*refs):
+    count = (len(refs) - 1) // 2
+    sem = refs[-1]
+    copies = [pltpu.make_async_copy(refs[i], refs[count + i], sem.at[i]) for i in range(count)]
+    for c in copies:
+        c.start()
+    for c in copies:
+        c.wait()
+
+
+def written(*arrays):
+    return pl.pallas_call(
+        write_kernel,
+        out_shape=tuple(jax.ShapeDtypeStruct(a.shape, a.dtype) for a in arrays),
+        in_specs=[pl.BlockSpec(memory_space=pltpu.VMEM)] * len(arrays),
+        out_specs=(pl.BlockSpec(memory_space=pl.ANY),) * len(arrays),
+        scratch_shapes=[pltpu.SemaphoreType.DMA((len(arrays),))],
+        compiler_params=pltpu.CompilerParams(vmem_limit_bytes=1024 * 1024),
+    )(*(pltpu.with_memory_space_constraint(a, pltpu.VMEM) for a in arrays))
 
 
 def fused(tp, dp, tokens, gain, w_query, w_key, w_value, w_outgate, w_in, w_fg, bias, w_output, mem, norm, peak):
@@ -342,22 +375,27 @@
     group, own_heads = rows // feats, vcols // DV
     heads = peak.shape[2]
     width = 2 * w_query.shape[2] + 2 * vcols
-    anywhere, vmem = pl.BlockSpec(memory_space=pl.ANY), pl.BlockSpec(memory_space=pltpu.VMEM)
+    vmem = pl.BlockSpec(memory_space=pltpu.VMEM)
     f32, bf16 = jnp.float32, jnp.bfloat16
     dma = pltpu.SemaphoreType.DMA
-    big = (w_query, w_key, w_value, w_outgate, w_in, w_fg, w_output, mem)
+    w_in, w_fg = jnp.swapaxes(w_in, 1, 2), jnp.swapaxes(w_fg, 1, 2)
+    arrays = (tokens, gain, w_query, w_key, w_value, w_outgate, w_in, w_fg, bias, w_output, mem, norm, peak)
+    gates = (BLOCKS, 2 * heads, rows)
+    big = (w_query.shape, w_key.shape, w_value.shape, w_outgate.shape, gates, w_output.shape)
+    lanes = -(-(2 * heads + 1) // 128) * 128
     others = max(dp - 1, 1)
-    mixed, new_mem, new_norm, new_peak = pl.pallas_call(
+    results = pl.pallas_call(
         functools.partial(fused_kernel, tp, dp),
         out_shape=(
-            jax.ShapeDtypeStruct(tokens.shape, tokens.dtype),
-            jax.ShapeDtypeStruct(mem.shape, mem.dtype),
-            jax.ShapeDtypeStruct((BLOCKS, heads, seqs, DK), f32),
-            jax.ShapeDtypeStruct(peak.shape, f32),
+            pltpu.VMEM(tokens.shape, tokens.dtype),
+            pltpu.VMEM(mem.shape, mem.dtype),
+            pltpu.VMEM(norm.shape, f32),
+            pltpu.VMEM(peak.shape, f32),
         ),
-        in_specs=[vmem, vmem] + [anywhere] * 6 + [vmem, anywhere, anywhere, vmem, vmem],
-        out_specs=(vmem, anywhere, vmem, vmem),
-        scratch_shapes=[pltpu.VMEM(w.shape, w.dtype) for w in big]
+        in_specs=[pl.BlockSpec(memory_space=pltpu.HBM)] * len(arrays),
+        out_specs=(vmem, vmem, vmem, vmem),
+        scratch_shapes=[pltpu.VMEM(shape, bf16) for shape in big]
+        + [pltpu.VMEM(a.shape, a.dtype) for a in (gain, bias, norm, peak)]
         + [
             pltpu.VMEM((BLOCKS, seqs, feats), bf16),
             pltpu.VMEM((BLOCKS, dp, group, seqs, feats), bf16),
@@ -365,13 +403,13 @@
             pltpu.VMEM((BLOCKS, dp, group, seqs, vcols), bf16),
             pltpu.VMEM((BLOCKS, dp, seqs, width), WIRE),
             pltpu.VMEM((BLOCKS, others, seqs, width), WIRE),
-            pltpu.VMEM((BLOCKS, dp, 3, seqs, 128), f32),
-            pltpu.VMEM((BLOCKS, others, 3, seqs, 128), f32),
+            pltpu.VMEM((BLOCKS, dp, seqs, lanes), f32),
+            pltpu.VMEM((BLOCKS, others, seqs, lanes), f32),
             pltpu.VMEM((BLOCKS, dp, seqs, feats), f32),
             pltpu.VMEM((BLOCKS, others, seqs, feats), f32),
             pltpu.VMEM((BLOCKS, tp, own_heads, seqs, DK), f32),
+            dma((5,)),
             dma((BLOCKS, 8)),
-            dma((BLOCKS,)),
             dma((BLOCKS, tp)),
             dma((BLOCKS, dp, group)),
             dma((BLOCKS, tp)),
@@ -383,9 +421,11 @@
             dma((BLOCKS, tp)),
             dma((BLOCKS, tp)),
         ],
-        compiler_params=pltpu.CompilerParams(has_side_effects=True, vmem_limit_bytes=60 * 1024 * 1024),
-    )(tokens, gain, w_query, w_key, w_value, w_outgate, w_in, w_fg, bias, w_output, mem, norm, peak)
-    return mixed, new_mem, jnp.transpose(new_norm, (0, 2, 1, 3)), new_peak
+        compiler_params=pltpu.CompilerParams(
+            collective_id=0, has_side_effects=True, vmem_limit_bytes=24 * 1024 * 1024
+        ),
+    )(*(pltpu.with_memory_space_constraint(a, pltpu.HBM) for a in arrays))
+    return written(*results)
 
 
 def whole_heads(tp, dp, *args):

time: 55.7 us -> 42.9 us (0.77)
  local copies, waits for them, and re-layouts: 11.8 us -> 0 us
  Pallas kernels: 43 us -> 42.1 us
    unnamed x8 -> x0, local copies, waits for them, and re-layouts: 11.8 us -> none
    pallas_call x1 -> x2, Pallas kernels: 43 us -> 42.1 us  [the longest x1 40 us: fused(): pl.pallas_call(functools.partial(fused_kernel, tp, dp), out_shape=(pltpu....]
where the time goes in v2:
time: 42.9 us; the launch traced here: 42.8 us
  Pallas kernels  42.1 us (98%)
  between operations  0.64 us (1%)
    pallas_call x1, Pallas kernels, fused(): pl.pallas_call(functools.partial(fused_kernel, tp, dp), out_shape=(pltpu....  40 us
    pallas_call x1, Pallas kernels, written(): pl.pallas_call(write_kernel, out_shape=tuple((jax.ShapeDtypeStruct(a.shap...  2.08 us

profile of v2, /device:TPU:0, one launch (start us, length us, event | category | flops | bytes accessed | tf_op | source)
XLA Modules:
  0.0 42.8 jit_solution(15574236243648338457)
XLA Ops:
  0.6 40.0 %shard_map.156 = (bf16[8,512]{1,0:T(8,128)(2,1)S(1)}, f32[2,8,512,128]{3,2,1,0:T(8,128)S(1)}, f32[2,8,16,128]{3,2,1,0:T(8,128)S(1)}, f32[2,8,16]{2,1,0:T(8,128)S(1)}) custom-call(bf16[8,512]{1,0:T(8,128)(2,1)} %tokens.1, f32[2,4096]{1,0:T(2,128)} %gain_in.1, bf16[2,1024,256]{2,1,0:T(8,128)(2,1)} %w_query.1, bf16[2,1024,256]{2,1,0:T(8,128)(2,1)} %w_key.1, ...), custom_call_target="tpu_custom_call" | custom-call | tf_op jit(solution)/shard_map/pallas_call | solution.py:387
  40.7 2.1 %shard_map.157 = (bf16[8,512]{1,0:T(8,128)(2,1)}, f32[2,8,512,128]{3,2,1,0:T(8,128)}, f32[2,8,16,128]{3,2,1,0:T(8,128)}, f32[2,8,16]{2,1,0:T(8,128)}) custom-call(bf16[8,512]{1,0:T(8,128)(2,1)S(1)} %get-tuple-element.8.refs_0_, f32[2,8,512,128]{3,2,1,0:T(8,128)S(1)} %get-tuple-element.9.refs_1_, f32[2,8,16,128]{3,2,1,0:T(8,128)S(1)} %get-tuple-element.10.refs_2_, ...), custom_call_target="tpu_custom_call" | custom-call | tf_op jit(solution)/shard_map/pallas_call | solution.py:362

commit v3 on v2

--- a/solution.py
+++ b/solution.py
@@ -320,7 +320,7 @@
             axis=1,
         )
         loads[b, 7].wait()
-        up = jnp.dot(gated, wp[b], preferred_element_type=f32)
+        up = jnp.dot(gated, wp[b], preferred_element_type=f32).astype(WIRE)
         for dd in range(dp):
             up_part[b, dd] = up[dd * seqs : (dd + 1) * seqs]
         flat = (slice(None), slice(None))
@@ -405,8 +405,8 @@
             pltpu.VMEM((BLOCKS, others, seqs, width), WIRE),
             pltpu.VMEM((BLOCKS, dp, seqs, lanes), f32),
             pltpu.VMEM((BLOCKS, others, seqs, lanes), f32),
-            pltpu.VMEM((BLOCKS, dp, seqs, feats), f32),
-            pltpu.VMEM((BLOCKS, others, seqs, feats), f32),
+            pltpu.VMEM((BLOCKS, dp, seqs, feats), WIRE),
+            pltpu.VMEM((BLOCKS, others, seqs, feats), WIRE),
             pltpu.VMEM((BLOCKS, tp, own_heads, seqs, DK), f32),
             dma((5,)),
             dma((BLOCKS, 8)),

time: 42.9 us -> 42.5 us (level)
  no operation moved by 1% of the time
where the time goes in v3:
time: 42.5 us; the launch traced here: 42.4 us
  Pallas kernels  41.7 us (98%)
  between operations  0.64 us (2%)
    pallas_call x1, Pallas kernels, fused(): pl.pallas_call(functools.partial(fused_kernel, tp, dp), out_shape=(pltpu....  39.6 us
    pallas_call x1, Pallas kernels, written(): pl.pallas_call(write_kernel, out_shape=tuple((jax.ShapeDtypeStruct(a.shap...  2.08 us

profile of v3, /device:TPU:0, one launch (start us, length us, event | category | flops | bytes accessed | tf_op | source)
XLA Modules:
  0.0 42.4 jit_solution(16701509978820176)
XLA Ops:
  0.6 39.6 %shard_map.156 = (bf16[8,512]{1,0:T(8,128)(2,1)S(1)}, f32[2,8,512,128]{3,2,1,0:T(8,128)S(1)}, f32[2,8,16,128]{3,2,1,0:T(8,128)S(1)}, f32[2,8,16]{2,1,0:T(8,128)S(1)}) custom-call(bf16[8,512]{1,0:T(8,128)(2,1)} %tokens.1, f32[2,4096]{1,0:T(2,128)} %gain_in.1, bf16[2,1024,256]{2,1,0:T(8,128)(2,1)} %w_query.1, bf16[2,1024,256]{2,1,0:T(8,128)(2,1)} %w_key.1, ...), custom_call_target="tpu_custom_call" | custom-call | tf_op jit(solution)/shard_map/pallas_call | solution.py:387
  40.3 2.1 %shard_map.157 = (bf16[8,512]{1,0:T(8,128)(2,1)}, f32[2,8,512,128]{3,2,1,0:T(8,128)}, f32[2,8,16,128]{3,2,1,0:T(8,128)}, f32[2,8,16]{2,1,0:T(8,128)}) custom-call(bf16[8,512]{1,0:T(8,128)(2,1)S(1)} %get-tuple-element.8.refs_0_, f32[2,8,512,128]{3,2,1,0:T(8,128)S(1)} %get-tuple-element.9.refs_1_, f32[2,8,16,128]{3,2,1,0:T(8,128)S(1)} %get-tuple-element.10.refs_2_, ...), custom_call_target="tpu_custom_call" | custom-call | tf_op jit(solution)/shard_map/pallas_call | solution.py:362
